TPU v7x, 512 devices: a whole 4x8x8 slice. The times are simulated.
512 devices in a mesh: sp: 128 (over z, y, core), tp: 4 (over x).
Axes of the slice: x: 4, y: 8, z: 8, core: 2. Of those that a mesh axis runs over, the one named last changes fastest.
Arguments:
- tokens: bfloat16 [24576, 2048], P('sp'), may hold values from -10 to 10
- w_query: bfloat16 [2048, 1024], P(None, 'tp'), may hold values from -0.125 to 0.125
- w_key: bfloat16 [2048, 256], P(None, 'tp'), may hold values from -0.125 to 0.125
- w_value: bfloat16 [2048, 256], P(None, 'tp'), may hold values from -0.125 to 0.125
- w_output: bfloat16 [1024, 2048], P('tp'), may hold values from -0.1875 to 0.1875
- query_gain: float32 [64], replicated, may hold values from 0.4 to 9
- key_gain: float32 [64], replicated, may hold values from 0.4 to 9
Outputs:
- mixed_out: bfloat16 [24576, 2048], P(('sp', 'tp'))
- log_sums: float32 [16, 24576], P('tp', 'sp')
All inputs are finite; a program needn't handle non-finite values.
Results may differ from a plain program's by a relative error of at most 0.009.
The roundings to bfloat16 on the way count: a program that leaves them out, or rounds other values in their place, can miss the bound.
Values may be sent and summed in bfloat16 or wider, within the bound.
A program may use at most 64 MiB of HBM per device.

v0:
```python
import math
import jax
import jax.numpy as jnp
from jax import lax
from jax.sharding import PartitionSpec as P

GRID_W = 64
ROPE_BASE = 10000.0
NORM_EPS = 1e-06


def in_blocks(x, dim, peers):
    shape = x.shape
    tiles = x.reshape(*shape[:dim], peers, shape[dim] // peers, *shape[dim + 1 :])
    return jnp.moveaxis(tiles, dim, 0)


def sum_at_owner(x, axis, dim):
    tiles = in_blocks(x, dim, lax.axis_size(axis))
    arrived = lax.all_to_all(tiles, axis, split_axis=0, concat_axis=0, tiled=True)
    return arrived.sum(axis=0)


def rotate(values, position):
    dim = values.shape[-1]
    half_dim = dim // 2
    inverse = ROPE_BASE ** (-jnp.arange(half_dim, dtype=jnp.float32) * (2.0 / dim))
    angles = position.astype(jnp.float32)[:, None] * inverse[None, :]
    cosine = jnp.cos(angles)[:, None, :]
    sine = jnp.sin(angles)[:, None, :]
    first_half = values[..., :half_dim]
    second_half = values[..., half_dim:]
    return jnp.concatenate(
        [first_half * cosine - second_half * sine, second_half * cosine + first_half * sine], -1
    )


def prepare(projected, gain_vec, grid_row, grid_col):
    values = projected.astype(jnp.float32)
    values = values * lax.rsqrt(jnp.mean(values * values, -1, keepdims=True) + NORM_EPS) * gain_vec
    split_at = values.shape[-1] // 2
    turned = jnp.concatenate(
        [rotate(values[..., :split_at], grid_row), rotate(values[..., split_at:], grid_col)], -1
    )
    return turned.astype(jnp.bfloat16)


def shards(tokens, w_query, w_key, w_value, w_output, query_gain, key_gain):
    head_dim = query_gain.shape[0]
    n_query = w_query.shape[1]
    n_key = w_key.shape[1]
    combined = jnp.concatenate([w_query, w_key, w_value], axis=1)
    projected = jnp.dot(tokens, combined, preferred_element_type=jnp.float32).astype(jnp.bfloat16)
    seq_rows = projected.shape[0]
    local_heads = n_query // head_dim
    local_kv = n_key // head_dim
    group_size = local_heads // local_kv
    positions = lax.axis_index("sp") * seq_rows + jnp.arange(seq_rows, dtype=jnp.int32)
    grid_row = positions // GRID_W
    grid_col = positions % GRID_W
    queries = prepare(
        projected[:, :n_query].reshape(seq_rows, local_heads, head_dim),
        query_gain,
        grid_row,
        grid_col,
    )
    key_rows = prepare(
        projected[:, n_query : n_query + n_key].reshape(seq_rows, local_kv, head_dim),
        key_gain,
        grid_row,
        grid_col,
    )
    key_value = jnp.concatenate(
        [key_rows.reshape(seq_rows, n_key), projected[:, n_query + n_key :]], axis=1
    )
    grouped = queries.reshape(seq_rows, local_kv, group_size, head_dim).transpose(1, 2, 0, 3)
    grouped = grouped.reshape(local_kv, group_size * seq_rows, head_dim)
    score_scale = head_dim ** (-0.5)
    initial = (
        jnp.full((local_kv, group_size * seq_rows), -1e30, jnp.float32),
        jnp.zeros((local_kv, group_size * seq_rows), jnp.float32),
        jnp.zeros((local_kv, group_size * seq_rows, head_dim), jnp.float32),
    )
    gathered = lax.all_gather(key_value, "sp", axis=0, tiled=True)
    piece_rows = gathered.shape[0]
    span_rows = math.gcd(piece_rows, 1024)
    pieces = gathered.reshape(piece_rows // span_rows, span_rows, 2, local_kv, head_dim)

    def update(state, block):
        running, totals, weighted = state
        key_block = block[:, 0]
        value_block = block[:, 1]
        scores = (
            jnp.einsum("kqd,skd->kqs", grouped, key_block, preferred_element_type=jnp.float32)
            * score_scale
        )
        new_max = jnp.maximum(running, jnp.max(scores, -1))
        shrink = jnp.exp(running - new_max)
        expos = jnp.exp(scores - new_max[..., None])
        totals = totals * shrink + jnp.sum(expos, -1)
        weighted = weighted * shrink[..., None] + jnp.einsum(
            "kqs,skd->kqd",
            expos.astype(jnp.bfloat16),
            value_block,
            preferred_element_type=jnp.float32,
        )
        return ((new_max, totals, weighted), None)

    result, unused = lax.scan(update, initial, pieces)
    running, totals, weighted = result
    attended = (weighted / totals[..., None]).astype(jnp.bfloat16)
    attended = (
        attended.reshape(local_kv, group_size, seq_rows, head_dim)
        .transpose(2, 0, 1, 3)
        .reshape(seq_rows, n_query)
    )
    log_sums = (running + jnp.log(totals)).reshape(local_heads, seq_rows)
    mixed_out = sum_at_owner(
        jnp.dot(attended, w_output, preferred_element_type=jnp.float32), "tp", 0
    ).astype(jnp.bfloat16)
    return (mixed_out, log_sums)


def solution(mesh):
    placed = (P("sp", None), P(None, "tp"), P(None, "tp"), P(None, "tp"), P("tp", None), P(), P())
    return jax.shard_map(
        shards,
        mesh=mesh,
        in_specs=placed,
        out_specs=(P(("sp", "tp"), None), P("tp", "sp")),
        check_vma=False,
    )
```

profile of v0, /device:TPU:1, one launch (start us, length us, event | category | flops | bytes accessed | tf_op | source)
XLA Modules:
  0.0 347.7 jit_solution(5974512695529500345)
XLA Ops:
  14.2 91.3 %all-gather.2.cloned.1.call-done = bf16[24576,128]{1,0:T(8,128)(2,1)} async-done(((bf16[192,128]{1,0:T(8,128)(2,1)}), bf16[24576,128]{1,0:T(8,128)(2,1)}) %all-gather.2.cloned.1.call-update) | async-done | bytes 6291472 | tf_op jit(solution)/shard_map/all_gather | solution.py:84
  105.5 21.6 %reshape.404 = bf16[24,1024,2,1,64]{4,2,1,0,3:T(2,128)(2,1)} reshape(bf16[24576,128]{1,0:T(8,128)(2,1)} %all-gather.2.cloned.1.call-done) | data formatting | bytes 12582912 | tf_op jit(solution)/shard_map/reshape | solution.py:87
  127.1 26.0 %copy.41 = bf16[24,1024,2,1,64]{1,4,3,2,0:T(8,128)(2,1)} copy(bf16[24,1024,2,1,64]{4,2,1,0,3:T(2,128)(2,1)} %reshape.404) | data formatting | bytes 12582912
  153.0 160.7 %while.15 = (s32[]{:T(128)}, f32[1,768]{1,0:T(1,128)S(1)}, f32[1,768]{1,0:T(1,128)S(1)}, f32[1,768,64]{1,2,0:T(8,128)S(1)}, bf16[24,1024,2,1,64]{1,4,3,2,0:T(8,1...) while((s32[]{:T(128)}, f32[1,768]{1,0:T(1,128)S(1)}, ...), condition=%wide.region_5.6_spmd.clone, body=%wide.region_2.5_spmd.clone.sunk | while | flops 207770112 | bytes 23450752 | solution.py:109
  156.3 2.7 fusion.70
  176.4 2.7 fusion.70
  183.1 2.7 fusion.70
  189.8 2.7 fusion.70
  196.5 2.7 fusion.70
  203.2 2.7 fusion.70
  209.9 2.7 fusion.70
  216.6 2.7 fusion.70
  223.3 2.7 fusion.70
  229.9 2.7 fusion.70
  236.6 2.7 fusion.70
  243.3 2.7 fusion.70
  250.0 2.7 fusion.70
  256.7 2.7 fusion.70
  270.1 2.7 fusion.70
  283.5 2.7 fusion.70
  296.9 2.7 fusion.70
  310.3 2.7 fusion.70
  315.8 4.0 %all-to-all-start = ((f32[4,48,2048]{2,1,0:T(8,128)}), f32[4,48,2048]{2,1,0:T(8,128)S(1)}, u32[]{:S(2)}, u32[]{:S(2)}) async-start(f32[4,48,2048]{2,1,0:T(8,128)} %fusion.28), calls=%async_computation | async-start | bytes 3145728 | tf_op jit(solution)/shard_map/all_to_all | solution.py:20
  320.5 19.6 %all-to-all-done = f32[4,48,2048]{2,1,0:T(8,128)S(1)} async-done(((f32[4,48,2048]{2,1,0:T(8,128)}), f32[4,48,2048]{2,1,0:T(8,128)S(1)}, u32[]{:S(2)}, u32[]{:S(2)}) %all-to-all-start) | async-done | bytes 1572896 | tf_op jit(solution)/shard_map/all_to_all | solution.py:20
  (238 shorter events, 121.2 us)
Async XLA Ops:
  7.2 307.1 %copy-start = (bf16[256,2048]{1,0:T(8,128)(2,1)S(1)}, bf16[256,2048]{1,0:T(8,128)(2,1)}, u32[]{:S(2)}) copy-start(bf16[256,2048]{1,0:T(8,128)(2,1)} %param.13) | copy-start | bytes 3145732
  7.2 98.3 %all-gather.2.cloned.1.call-start = ((), (), s32[]{:S(2)}) async-start(), calls=%async_computation.1 | async-start | bytes 6340608 | tf_op jit(solution)/shard_map/all_gather | solution.py:84
  9.8 4.1 %copy-start.3 = (f32[64]{0:T(128)S(1)}, f32[64]{0:T(128)}, u32[]{:S(2)}) copy-start(f32[64]{0:T(128)} %param.14) | copy-start | bytes 772
  156.3 2.8 copy-start.1
  163.0 2.8 copy-start.1
  169.7 2.8 copy-start.1
  176.4 2.8 copy-start.1
  183.1 2.8 copy-start.1
  189.7 2.8 copy-start.1
  196.4 2.8 copy-start.1
  203.1 2.8 copy-start.1
  209.8 2.8 copy-start.1
  216.5 2.8 copy-start.1
  223.2 2.8 copy-start.1
  229.9 2.8 copy-start.1
  236.6 2.8 copy-start.1
  243.3 2.8 copy-start.1
  250.0 2.8 copy-start.1
  256.7 2.8 copy-start.1
  263.4 2.8 copy-start.1
  270.1 2.8 copy-start.1
  276.8 2.8 copy-start.1
  283.5 2.8 copy-start.1
  315.8 24.2 %all-to-all-start = ((f32[4,48,2048]{2,1,0:T(8,128)}), f32[4,48,2048]{2,1,0:T(8,128)S(1)}, u32[]{:S(2)}, u32[]{:S(2)}) async-start(f32[4,48,2048]{2,1,0:T(8,128)} %fusion.28), calls=%async_computation | async-start | bytes 3145728 | tf_op jit(solution)/shard_map/all_to_all | solution.py:20
  (5 other events, 13.7 us)
Sparse Core Ops, SparseCore 0:
  13.7 91.7 all-gather.1
where the time goes:
time: 350 us; the launch traced here: 348 us
  matrix products  124 us (35%)
  waiting for transfers between devices  111 us (32%)
  local copies, waits for them, and re-layouts  77.4 us (22%)
  other arithmetic  16.5 us (5%)
  between operations  14.2 us (4%)
  starting transfers between devices  4 us (1%)
    all_gather x1, waiting for transfers between devices, shards(): gathered = lax.all_gather(key_value, 'sp', axis=0, tiled=True)  91.3 us
    dot_general x24, matrix products, update(): jnp.einsum('kqs,skd->kqd', expos.astype(jnp.bfloat16), value_block, prefe...  65.3 us
    dot_general x24, matrix products, update(): jnp.einsum('kqd,skd->kqs', grouped, key_block, preferred_element_type=jnp...  54.7 us
    unnamed x10, local copies, waits for them, and re-layouts  28.7 us
    squeeze x24, local copies, waits for them, and re-layouts, shards(): result, unused = lax.scan(update, initial, pieces)  23.3 us
    reshape x1, local copies, waits for them, and re-layouts, shards(): gathered.reshape(piece_rows // span_rows, span_rows, 2, local_kv, head_dim)  21.6 us
    all_to_all x1, waiting for transfers between devices, sum_at_owner(): lax.all_to_all(tiles, axis, split_axis=0, concat_axis=0, tiled=True)  19.6 us
    reduce_sum x24, other arithmetic, update(): totals = totals * shrink + jnp.sum(expos, -1)  13.4 us
  transfers between devices with their start and end apart: 2, of which 2 were waited for; matrix products, arithmetic and copies ran while one was open for 0% of the time, Pallas kernels for 0%

commit v1 on v0

--- a/solution.py
+++ b/solution.py
@@ -3,6 +3,7 @@
 import jax.numpy as jnp
 from jax import lax
 from jax.sharding import PartitionSpec as P
+from jax.lax import all_to_all, psum
 
 GRID_W = 64
 ROPE_BASE = 10000.0
@@ -81,7 +82,14 @@
         jnp.zeros((local_kv, group_size * seq_rows), jnp.float32),
         jnp.zeros((local_kv, group_size * seq_rows, head_dim), jnp.float32),
     )
-    gathered = lax.all_gather(key_value, "sp", axis=0, tiled=True)
+
+    def targets_change(mat, axis_no):
+        r2 = psum(1, "sp")
+        x_next = jnp.stack([mat] * r2, axis=0)
+        later = all_to_all(x_next, "sp", 0, 0)
+        return jnp.concatenate(later, axis=axis_no)
+
+    gathered = targets_change(key_value, 0)
     piece_rows = gathered.shape[0]
     span_rows = math.gcd(piece_rows, 1024)
     pieces = gathered.reshape(piece_rows // span_rows, span_rows, 2, local_kv, head_dim)

time: 350 us -> 441 us (1.26)
  the two profiles are of different devices: /device:TPU:1 before, /device:TPU:17 now
where the time goes in v1:
time: 441 us; the launch traced here: 439 us
  waiting for transfers between devices  193 us (44%)
  matrix products  124 us (28%)
  local copies, waits for them, and re-layouts  81 us (18%)
  starting transfers between devices  22.1 us (5%)
  other arithmetic  16.5 us (4%)
    all_to_all x1, waiting for transfers between devices, targets_change(): later = all_to_all(x_next, 'sp', 0, 0)  176 us
    dot_general x24, matrix products, update(): jnp.einsum('kqs,skd->kqd', expos.astype(jnp.bfloat16), value_block, prefe...  65.3 us
    dot_general x24, matrix products, update(): jnp.einsum('kqd,skd->kqs', grouped, key_block, preferred_element_type=jnp...  54.7 us
    unnamed x10, local copies, waits for them, and re-layouts  28.7 us
    squeeze x24, local copies, waits for them, and re-layouts, shards(): result, unused = lax.scan(update, initial, pieces)  23.3 us
    another operation x1, local copies, waits for them, and re-layouts, shards(): gathered.reshape(piece_rows // span_rows, span_rows, 2, local_kv, head_dim)  21.6 us
    all_to_all x1, starting transfers between devices, targets_change(): later = all_to_all(x_next, 'sp', 0, 0)  18.1 us
    all_to_all x1, waiting for transfers between devices, sum_at_owner(): lax.all_to_all(tiles, axis, split_axis=0, concat_axis=0, tiled=True)  17.5 us
  transfers between devices with their start and end apart: 2, of which 2 were waited for; matrix products, arithmetic and copies ran while one was open for 0% of the time, Pallas kernels for 0%

profile of v1, /device:TPU:17, one launch (start us, length us, event | category | flops | bytes accessed | tf_op | source)
XLA Modules:
  0.0 438.5 jit_solution(3904720473924441146)
XLA Ops:
  6.4 4.2 stack.2
  10.6 18.1 %all-to-all-start = ((bf16[128,192,128]{2,1,0:T(8,128)(2,1)}), bf16[128,192,128]{2,1,0:T(8,128)(2,1)}, u32[]{:S(2)}, u32[]{:S(2)}) async-start(bf16[128,192,128]{2,1,0:T(8,128)(2,1)} %stack.2), calls=%async_computation | async-start | bytes 12582912 | tf_op jit(solution)/shard_map/all_to_all | solution.py:89
  29.3 175.9 %all-to-all-done = bf16[128,192,128]{2,1,0:T(8,128)(2,1)} async-done(((bf16[128,192,128]{2,1,0:T(8,128)(2,1)}), bf16[128,192,128]{2,1,0:T(8,128)(2,1)}, u32[]{:S(2)}, u32[]{:S(2)}) %all-to-all-start) | async-done | bytes 6291488 | tf_op jit(solution)/shard_map/all_to_all | solution.py:89
  205.2 21.6 %reshape.402 = bf16[24,1024,2,1,64]{4,2,1,0,3:T(2,128)(2,1)} reshape(bf16[128,192,128]{2,1,0:T(8,128)(2,1)} %all-to-all-done) | data formatting | bytes 12582912 | tf_op jit(solution)/shard_map/reshape;reshape | solution.py:95
  226.8 26.0 %copy.41 = bf16[24,1024,2,1,64]{1,4,3,2,0:T(8,128)(2,1)} copy(bf16[24,1024,2,1,64]{4,2,1,0,3:T(2,128)(2,1)} %reshape.402) | data formatting | bytes 12582912
  252.7 160.7 %while.15 = (s32[]{:T(128)}, f32[1,768]{1,0:T(1,128)S(1)}, f32[1,768]{1,0:T(1,128)S(1)}, f32[1,768,64]{1,2,0:T(8,128)S(1)}, bf16[24,1024,2,1,64]{1,4,3,2,0:T(8,1...) while((s32[]{:T(128)}, f32[1,768]{1,0:T(1,128)S(1)}, ...), condition=%wide.region_5.6_spmd.clone, body=%wide.region_2.5_spmd.clone.sunk | while | flops 207770112 | bytes 23450752 | solution.py:117
  256.0 2.7 fusion.70
  262.7 2.7 fusion.70
  269.4 2.7 fusion.70
  276.1 2.7 fusion.70
  282.8 2.7 fusion.70
  289.5 2.7 fusion.70
  296.2 2.7 fusion.70
  302.9 2.7 fusion.70
  309.6 2.7 fusion.70
  322.9 2.7 fusion.70
  336.3 2.7 fusion.70
  349.7 2.7 fusion.70
  363.1 2.7 fusion.70
  376.5 2.7 fusion.70
  389.9 2.7 fusion.70
  403.3 2.7 fusion.70
  415.5 4.0 all-to-all-start.1
  420.2 17.5 %all-to-all-done.1 = f32[4,48,2048]{2,1,0:T(8,128)S(1)} async-done(((f32[4,48,2048]{2,1,0:T(8,128)}), f32[4,48,2048]{2,1,0:T(8,128)S(1)}, u32[]{:S(2)}, u32[]{:S(2)}) %all-to-all-start.1) | async-done | bytes 1572896 | tf_op jit(solution)/shard_map/all_to_all | solution.py:21
  (238 shorter events, 126.0 us)
Async XLA Ops:
  0.6 413.4 %copy-start = (bf16[256,2048]{1,0:T(8,128)(2,1)S(1)}, bf16[256,2048]{1,0:T(8,128)(2,1)}, u32[]{:S(2)}) copy-start(bf16[256,2048]{1,0:T(8,128)(2,1)} %param.13) | copy-start | bytes 3145732
  10.6 18.4 %copy-start.3 = (f32[64]{0:T(128)S(1)}, f32[64]{0:T(128)}, u32[]{:S(2)}) copy-start(f32[64]{0:T(128)} %param.14) | copy-start | bytes 772
  10.6 194.6 %all-to-all-start = ((bf16[128,192,128]{2,1,0:T(8,128)(2,1)}), bf16[128,192,128]{2,1,0:T(8,128)(2,1)}, u32[]{:S(2)}, u32[]{:S(2)}) async-start(bf16[128,192,128]{2,1,0:T(8,128)(2,1)} %stack.2), calls=%async_computation | async-start | bytes 12582912 | tf_op jit(solution)/shard_map/all_to_all | solution.py:89
  256.0 2.8 copy-start.1
  262.7 2.8 copy-start.1
  269.4 2.8 copy-start.1
  276.1 2.8 copy-start.1
  282.8 2.8 copy-start.1
  289.4 2.8 copy-start.1
  296.1 2.8 copy-start.1
  302.8 2.8 copy-start.1
  309.5 2.8 copy-start.1
  316.2 2.8 copy-start.1
  322.9 2.8 copy-start.1
  329.6 2.8 copy-start.1
  336.3 2.8 copy-start.1
  343.0 2.8 copy-start.1
  349.7 2.8 copy-start.1
  356.4 2.8 copy-start.1
  363.1 2.8 copy-start.1
  369.8 2.8 copy-start.1
  376.5 2.8 copy-start.1
  389.9 2.8 copy-start.1
  415.5 22.2 %all-to-all-start.1 = ((f32[4,48,2048]{2,1,0:T(8,128)}), f32[4,48,2048]{2,1,0:T(8,128)S(1)}, u32[]{:S(2)}, u32[]{:S(2)}) async-start(f32[4,48,2048]{2,1,0:T(8,128)} %fusion.28), calls=%async_computation.1 | async-start | bytes 3145728 | tf_op jit(solution)/shard_map/all_to_all | solution.py:21
  (5 other events, 13.7 us)
